TPU v7x, 32 devices: a whole 2x2x4 slice. The times are simulated.
32 devices in a mesh: row: 8 (over z, x), col: 4 (over y, core).
Axes of the slice: x: 2, y: 2, z: 4, core: 2. Of those that a mesh axis runs over, the one named last changes fastest.
Arguments:
- tokens: bfloat16 [9216, 4096], P('row'), may hold values from -6 to 6
- proj_in: bfloat16 [4096, 512], P(None, 'col'), may hold values from -0.09375 to 0.09375
- proj_out: bfloat16 [512, 4096], P(None, 'col'), may hold values from -0.25 to 0.25
Outputs:
- mixed: bfloat16 [9216, 4096], P('row', 'col')
All inputs are finite; a program needn't handle non-finite values.
Results may differ from a plain program's by a relative error of at most 0.0057.
Values may be sent and summed in bfloat16 or wider, within the bound.
A program may use at most 64 MiB of HBM per device.

v0:
```python
import functools
import math

import jax
import jax.numpy as jnp
import numpy as np
from jax import lax
from jax.experimental import pallas as pl
from jax.experimental.pallas import tpu as pltpu
from jax.sharding import PartitionSpec as P

MESH = pl.DeviceIdType.MESH


def up(value, step):
    return -(-value // step) * step


def plan(rows, devices):
    period = rows // 2
    piece = rows // (2 * devices)
    pad = up(piece, 8)
    share = period // (2 * devices)
    height = up(share + 1, 8)
    return period, piece, pad, share, height


@functools.lru_cache(maxsize=None)
def tables(rows, devices, group):
    period, piece, pad, share, height = plan(rows, devices)
    half = group // 2
    odd = np.arange(group) > half
    freq = np.where(odd, np.arange(group) - half, np.arange(group))
    angle = 2 * np.pi * (np.arange(group)[:, None] * freq[None, :] % group) / group
    chan = np.where(odd, np.sin(angle), np.cos(angle)) / math.sqrt(group)
    chan_hi = chan.astype(jnp.bfloat16)
    chan_lo = (chan - chan_hi.astype(np.float64)).astype(jnp.bfloat16)
    unpack = np.zeros((group, group))
    for col in range(group):
        f = freq[col]
        unpack[col, f] = -1.0 if odd[col] else 1.0
        unpack[col, (group - f) % group] = 1.0
    pos = np.arange(2 * pad)
    is_y = pos >= pad
    local = np.where(is_y, pos - pad, pos)
    valid = np.tile(local < piece, devices)
    m = (piece * np.arange(devices)[:, None] + local[None, :]).reshape(-1)
    is_y = np.tile(is_y, devices)
    k = (share * np.arange(devices)[:, None] + np.arange(height)[None, :])
    pair_m = 2 * np.where(is_y, period - 1 - m, m)
    self_m = 2 * m + is_y
    seq = []
    for twice_m in (self_m, pair_m):
        angle = np.pi * (twice_m[None, None, :] * k[:, :, None] % (2 * period)) / period
        both = np.stack([np.cos(angle), np.sin(angle)], axis=1) * valid
        seq.append(both.reshape(devices * 2 * height, -1))
    seq = np.stack(seq).astype(jnp.bfloat16)
    q = np.arange(2 * devices)[:, None]
    p = np.arange(devices)[None, :]
    angle = 2 * np.pi * (p * q % (2 * devices)) / (2 * devices)
    even_a, even_b = np.cos(angle), -np.sin(angle)
    odd_a, odd_b = np.sin(angle), np.cos(angle)
    for a, b in ((even_a, even_b), (odd_a, odd_b)):
        a[:, 0] = 1.0
        b[:, 0] = np.where(q[:, 0] % 2, -1.0, 1.0)
    even = np.stack([even_a, even_b], axis=2).reshape(2 * devices, 2 * devices, 1)
    oddc = np.stack([odd_a, odd_b], axis=2).reshape(2 * devices, 2 * devices, 1)
    coef = np.where(odd, oddc, even) / math.sqrt(rows * devices)
    order = np.zeros((period, devices * 2 * height))
    for row in range(period):
        mirrored = row > period // 2
        kk = period - row if mirrored else row
        s = min(kk // share, devices - 1)
        order[row, s * 2 * height + mirrored * height + kk - s * share] = 1.0
    return (
        np.stack([chan_hi, chan_lo]),
        unpack.astype(jnp.bfloat16),
        seq,
        coef.astype(np.float32),
        order.astype(jnp.bfloat16),
    )


def cos_sin_small(x):
    square = x * x
    cos_sum, sin_sum = jnp.zeros_like(x), jnp.zeros_like(x)
    for j in range(8, -1, -1):
        sign = -1.0 if j % 2 else 1.0
        cos_sum = cos_sum * square + sign / math.factorial(2 * j)
        sin_sum = sin_sum * square + sign / math.factorial(2 * j + 1)
    return cos_sum, sin_sum * x


def kernel(
    devices, cols, chunks,
    tok_hbm, pin_hbm, pout_hbm, chan_hbm, unpack_hbm, seq_hbm, coef_hbm, order_hbm,
    out_ref,
    tok, pin, pout, chan, unpack, seq, coef, order,
    packed, wide, slot1, send1, recv1, mid, send2, recv2, twc, tws, parts, send3, recv3, weight,
    tok_sem, in_sem, ssem1, rsem1, ssem2, rsem2, ssem3, rsem3, gsem, ysem, psem,
):
    me = lax.axis_index("row")
    col = lax.axis_index("col")
    partner = col + 1 - 2 * lax.rem(col, 2)
    rows, group = packed.shape
    period, piece, pad, share, height = plan(rows, devices)
    half = group // 2
    f32, bf16 = jnp.float32, jnp.bfloat16
    chips = cols // 2

    def peer_row(d):
        return lax.rem(me + d, devices)

    def peer_col(j):
        return lax.rem(col + 2 * j, cols)

    barrier = pltpu.get_barrier_semaphore()

    step = rows // chunks
    tok_copies = [
        pltpu.make_async_copy(
            tok_hbm.at[pl.ds(i * step, step)], tok.at[pl.ds(i * step, step)], tok_sem.at[i]
        )
        for i in range(chunks)
    ]
    loads = [
        pltpu.make_async_copy(src, dst, in_sem.at[i])
        for i, (src, dst) in enumerate(
            [
                (pin_hbm, pin),
                (chan_hbm, chan),
                (seq_hbm.at[jnp.minimum(me, 1)], seq),
                (pout_hbm, pout),
                (unpack_hbm, unpack),
                (coef_hbm, coef),
                (order_hbm, order),
            ]
        )
    ]
    loads[0].start()
    loads[1].start()
    for copy in tok_copies:
        copy.start()
    for copy in loads[2:]:
        copy.start()

    def greet(d, _):
        pl.semaphore_signal(barrier, inc=1, device_id={"row": peer_row(d)}, device_id_type=MESH)
        return 0

    lax.fori_loop(1, devices, greet, 0)
    pl.semaphore_signal(barrier, inc=1, device_id={"col": partner}, device_id_type=MESH)
    for j in range(1, chips):
        pl.semaphore_signal(barrier, inc=1, device_id={"col": peer_col(j)}, device_id_type=MESH)

    shape = (devices, height, group)
    p_id = lax.broadcasted_iota(jnp.int32, shape, 0)
    k_id = lax.broadcasted_iota(jnp.int32, shape, 1) + share * me
    angle = (p_id * k_id).astype(f32) * (2.0 * math.pi / (rows * devices))
    cos_val, sin_val = cos_sin_small(angle)
    twc[...] = cos_val
    tws[...] = sin_val

    lane = lax.broadcasted_iota(jnp.int32, (1, group), 1)
    sign = jnp.where(lane > half, -1.0, 1.0).astype(f32)

    loads[0].wait()
    loads[1].wait()
    for i in range(chunks):
        tok_copies[i].wait()
        branch = jnp.dot(
            tok[i * step:(i + 1) * step, :], pin[...], preferred_element_type=f32
        ).astype(bf16)
        packed[i * step:(i + 1) * step, :] = jnp.dot(
            branch, chan[0], preferred_element_type=f32
        ) + jnp.dot(branch, chan[1], preferred_element_type=f32)

    pl.semaphore_wait(barrier, devices - 1 + 1 + chips - 1)

    if pad != piece:
        slot1[...] = jnp.zeros_like(slot1)
    for p in range(devices):
        other = 2 * devices - p if p else devices
        x = packed[pl.ds(p, piece, stride=2 * devices), :]
        y = packed[pl.ds(other, piece, stride=2 * devices), :]
        if p:
            y = y * sign
        if pad == piece:
            send1[p] = jnp.concatenate([x, y], axis=0).astype(bf16)
        else:
            slot1[0:piece, :] = x
            slot1[pad:pad + piece, :] = y
            send1[p] = slot1[...].astype(bf16)

    def remote(src, dst, ssem, rsem, target):
        return pltpu.make_async_remote_copy(
            src_ref=src, dst_ref=dst, send_sem=ssem, recv_sem=rsem,
            device_id=target, device_id_type=MESH,
        )

    def exchange1(d, slot):
        to = peer_row(d)
        return remote(send1.at[to], recv1.at[slot], ssem1.at[d], rsem1.at[slot], {"row": to})

    def start1(d, _):
        exchange1(d, me).start()
        return 0

    lax.fori_loop(1, devices, start1, 0)
    recv1[me] = send1[me]

    for copy in loads[2:]:
        copy.wait()
    for c in range(cols):
        weight[c * group:(c + 1) * group, :] = jnp.dot(
            unpack[...], pout[c * group:(c + 1) * group, :], preferred_element_type=f32
        ).astype(bf16)

    def wait1(d, _):
        exchange1(d, lax.rem(me + devices - d, devices)).wait_recv()
        return 0

    lax.fori_loop(1, devices, wait1, 0)

    data = recv1[...].astype(f32)
    is_y = lax.broadcasted_iota(jnp.int32, data.shape, 1) >= pad
    flat = (devices * 2 * pad, group)
    both = jnp.concatenate(
        [
            jnp.where(is_y, 0.0, data).astype(bf16).reshape(flat),
            jnp.where(is_y, data, 0.0).astype(bf16).reshape(flat),
        ],
        axis=1,
    )
    mid[...] = jnp.dot(seq[...], both, preferred_element_type=f32).reshape(mid.shape)
    first = me == 0
    odd_lane = lane > half

    def exchange2(d, slot):
        to = peer_row(d)
        return remote(send2.at[to], recv2.at[slot], ssem2.at[d], rsem2.at[slot], {"row": to})

    def start2(d, _):
        s = peer_row(d)
        top_x, top_y = mid[s, :height, :group], mid[s, :height, group:]
        low_x, low_y = mid[s, height:, :group], mid[s, height:, group:]
        a = jnp.where(first, jnp.where(odd_lane, low_x, top_x), top_x + top_y)
        b = jnp.where(first, jnp.where(odd_lane, low_y, top_y), low_x + low_y)
        send2[s] = jnp.concatenate([a, b], axis=0).astype(bf16)

        @pl.when(d < devices)
        def _():
            exchange2(d, me).start()

        return 0

    lax.fori_loop(1, devices + 1, start2, 0)
    recv2[me] = send2[me]

    def rotate(p):
        ab = recv2[p].astype(f32)
        a, b = ab[:height], ab[height:]
        cos_val, sin_val = twc[p], tws[p]
        parts[2 * p] = cos_val * a - sin_val * b
        parts[2 * p + 1] = sin_val * a + cos_val * b

    rotate(me)

    def wait2(d, _):
        src = lax.rem(me + devices - d, devices)
        exchange2(d, src).wait_recv()
        rotate(src)
        return 0

    lax.fori_loop(1, devices, wait2, 0)

    def exchange3(to, slot):
        return remote(send3.at[to], recv3.at[col, slot], ssem3.at[to], rsem3.at[slot], {"row": to})

    def outer(q):
        return jnp.sum(coef[q][:, None, :] * parts[...], axis=0)

    def send_to(to):
        @pl.when(to != me)
        def _():
            exchange3(to, me).start()

    def start3(i, _):
        for h in range(2):
            q = 2 * i + h
            direct = outer(q)
            mirror = outer(2 * devices - 1 - q)
            send3[i, h] = jnp.concatenate([direct, mirror * sign], axis=0).astype(bf16)
            send3[devices - 1 - i, 1 - h] = jnp.concatenate(
                [mirror, direct * sign], axis=0
            ).astype(bf16)
        send_to(i)
        send_to(devices - 1 - i)
        return 0

    lax.fori_loop(0, devices // 2, start3, 0)
    recv3[col, me] = send3[me]

    def to_partner(c, src):
        block = recv3.at[c, src]
        return remote(block, block, psem.at[c, src], gsem.at[c, src], {"col": partner})

    def to_chip(j, c, src):
        block = recv3.at[c, src]
        return remote(block, block, ysem.at[j, src], gsem.at[c, src], {"col": peer_col(j)})

    def forward(src):
        for j in range(1, chips):
            to_chip(j, col, src).start()
        to_partner(col, src).start()

    def relay(src):
        for j in range(1, chips):
            c = lax.rem(col + cols - 2 * j, cols)
            to_chip(j, c, src).wait_recv()
            to_partner(c, src).start()

    forward(me)

    def wait3(d, _):
        src = lax.rem(me + devices - d, devices)
        pltpu_wait = remote(
            send3.at[me], recv3.at[col, src], ssem3.at[me], rsem3.at[src], {"row": src}
        )
        pltpu_wait.wait_recv()
        forward(src)
        return 0

    lax.fori_loop(1, devices, wait3, 0)

    def relay_all(d, _):
        relay(lax.rem(me + devices - d, devices))
        return 0

    lax.fori_loop(0, devices, relay_all, 0)

    def wait_partner(d, _):
        src = lax.rem(me + devices - d, devices)
        for j in range(chips):
            c = lax.rem(partner + 2 * j, cols)
            to_partner(c, src).wait_recv()
        return 0

    lax.fori_loop(0, devices, wait_partner, 0)

    for h in range(2):
        arrived = jnp.concatenate(
            [recv3[c, :, h].reshape(devices * 2 * height, group) for c in range(cols)], axis=1
        )
        natural = jnp.dot(order[...], arrived, preferred_element_type=f32).astype(bf16)
        out_ref[h * period:(h + 1) * period, :] = jnp.dot(
            natural, weight[...], preferred_element_type=f32
        ).astype(bf16)

    def drain(d, _):
        exchange1(d, me).wait_send()
        exchange2(d, me).wait_send()
        exchange3(peer_row(d), me).wait_send()
        return 0

    lax.fori_loop(1, devices, drain, 0)

    def drain_gather(src, _):
        for j in range(1, chips):
            to_chip(j, col, src).wait_send()
        for j in range(chips):
            to_partner(peer_col(j), src).wait_send()
        return 0

    lax.fori_loop(0, devices, drain_gather, 0)


def solution(mesh):
    devices, cols = mesh.shape["row"], mesh.shape["col"]

    def on_device(tokens, proj_in, proj_out):
        rows, width = tokens.shape
        group = proj_in.shape[1]
        channels, out_cols = proj_out.shape
        period, piece, pad, share, height = plan(rows, devices)
        consts = tables(rows, devices, group)
        chunks = 8
        f32, bf16 = jnp.float32, jnp.bfloat16
        dma = pltpu.SemaphoreType.DMA
        seq_shape = consts[2].shape[1:]
        return pl.pallas_call(
            functools.partial(kernel, devices, cols, chunks),
            out_shape=jax.ShapeDtypeStruct((rows, out_cols), bf16),
            in_specs=[pl.BlockSpec(memory_space=pl.ANY)] * 8,
            out_specs=pl.BlockSpec(memory_space=pltpu.VMEM),
            scratch_shapes=[
                pltpu.VMEM((rows, width), bf16),
                pltpu.VMEM((width, group), bf16),
                pltpu.VMEM((channels, out_cols), bf16),
                pltpu.VMEM((2, group, group), bf16),
                pltpu.VMEM((group, group), bf16),
                pltpu.VMEM(seq_shape, bf16),
                pltpu.VMEM((2 * devices, 2 * devices, group), f32),
                pltpu.VMEM(consts[4].shape, bf16),
                pltpu.VMEM((rows, group), f32),
                pltpu.VMEM((8, group), f32),
                pltpu.VMEM((2 * pad, group), f32),
                pltpu.VMEM((devices, 2 * pad, group), bf16),
                pltpu.VMEM((devices, 2 * pad, group), bf16),
                pltpu.VMEM((devices, 2 * height, 2 * group), f32),
                pltpu.VMEM((devices, 2 * height, group), bf16),
                pltpu.VMEM((devices, 2 * height, group), bf16),
                pltpu.VMEM((devices, height, group), f32),
                pltpu.VMEM((devices, height, group), f32),
                pltpu.VMEM((2 * devices, height, group), f32),
                pltpu.VMEM((devices, 2, 2 * height, group), bf16),
                pltpu.VMEM((cols, devices, 2, 2 * height, group), bf16),
                pltpu.VMEM((channels, out_cols), bf16),
                dma((chunks,)),
                dma((7,)),
                dma((devices,)),
                dma((devices,)),
                dma((devices,)),
                dma((devices,)),
                dma((devices,)),
                dma((devices,)),
                dma((cols, devices)),
                dma((cols // 2, devices)),
                dma((cols, devices)),
            ],
            compiler_params=pltpu.CompilerParams(
                collective_id=0, has_side_effects=True, vmem_limit_bytes=60 * 2**20
            ),
            name="mix",
        )(tokens, proj_in, proj_out, *[jnp.asarray(c) for c in consts])

    return jax.shard_map(
        on_device,
        mesh=mesh,
        in_specs=(P("row", None), P(None, "col"), P(None, "col")),
        out_specs=P("row", "col"),
        check_vma=False,
    )
```

profile of v0, /device:TPU:17, one launch (start us, length us, event | category | flops | bytes accessed | tf_op | source)
XLA Modules:
  0.0 46.6 jit_solution(15600749859163200930)
XLA Ops:
  0.0 43.3 %mix.1 = bf16[1152,1024]{1,0:T(8,128)(2,1)} custom-call(bf16[1152,4096]{1,0:T(8,128)(2,1)} %tok_hbm.1, bf16[4096,128]{1,0:T(8,128)(2,1)} %pin_hbm.1, bf16[512,1024]{1,0:T(8,128)(2,1)} %pout_hbm.1, bf16[2,128,128]{2,1,0:T(8,128)(2,1)} %constant.10.clone.chan_hbm, bf16[128,128]{1,0:T(8,128)(2,1)} %constant.11.clone.unpack_hbm, ...), custom_call_target="tpu_custom_call" | custom-call | tf_op jit(solution)/shard_map/mix/pallas_call | solution.py:391
  43.3 3.3 %copy.10 = bf16[1152,1024]{1,0:T(8,128)(2,1)} copy(bf16[1152,1024]{1,0:T(8,128)(2,1)} %mix.1) | data formatting | bytes 4718592
where the time goes:
time: 46.7 us; the launch traced here: 46.6 us
  Pallas kernels  43.3 us (93%)
  local copies, waits for them, and re-layouts  3.27 us (7%)
    pallas_call x1, Pallas kernels, on_device(): pl.pallas_call(functools.partial(kernel, devices, cols, chunks), out_shap...  43.3 us
    unnamed x1, local copies, waits for them, and re-layouts  3.27 us

commit v1 on v0

--- a/solution.py
+++ b/solution.py
@@ -391,7 +391,7 @@
         return pl.pallas_call(
             functools.partial(kernel, devices, cols, chunks),
             out_shape=jax.ShapeDtypeStruct((rows, out_cols), bf16),
-            in_specs=[pl.BlockSpec(memory_space=pl.ANY)] * 8,
+            in_specs=[pl.BlockSpec(memory_space=pltpu.HBM)] * 8,
             out_specs=pl.BlockSpec(memory_space=pltpu.VMEM),
             scratch_shapes=[
                 pltpu.VMEM((rows, width), bf16),
@@ -429,10 +429,10 @@
                 dma((cols, devices)),
             ],
             compiler_params=pltpu.CompilerParams(
-                collective_id=0, has_side_effects=True, vmem_limit_bytes=60 * 2**20
+                collective_id=0, has_side_effects=True, vmem_limit_bytes=40 * 2**20
             ),
             name="mix",
-        )(tokens, proj_in, proj_out, *[jnp.asarray(c) for c in consts])
+        )(*[pltpu.with_memory_space_constraint(a, pltpu.HBM) for a in (tokens, proj_in, proj_out, *[jnp.asarray(c) for c in consts])])
 
     return jax.shard_map(
         on_device,

time: 46.7 us -> 43.1 us (0.923)
  local copies, waits for them, and re-layouts: 3.27 us -> 1.41 us
  Pallas kernels: 43.3 us -> 41.6 us
    unnamed x1, local copies, waits for them, and re-layouts: 3.27 us -> 1.41 us
    pallas_call x1, Pallas kernels: 43.3 us -> 41.6 us  [on_device(): pl.pallas_call(functools.partial(kernel, devices, cols, chunks), out_shap...]
where the time goes in v1:
time: 43.1 us; the launch traced here: 43 us
  Pallas kernels  41.6 us (97%)
  local copies, waits for them, and re-layouts  1.41 us (3%)
    pallas_call x1, Pallas kernels, on_device(): pl.pallas_call(functools.partial(kernel, devices, cols, chunks), out_shap...  41.6 us
    unnamed x1, local copies, waits for them, and re-layouts  1.41 us

profile of v1, /device:TPU:17, one launch (start us, length us, event | category | flops | bytes accessed | tf_op | source)
XLA Modules:
  0.0 43.0 jit_solution(3775894019852735487)
XLA Ops:
  0.0 41.6 %mix.1 = bf16[1152,1024]{1,0:T(8,128)(2,1)S(1)} custom-call(bf16[1152,4096]{1,0:T(8,128)(2,1)} %tok_hbm.1, bf16[4096,128]{1,0:T(8,128)(2,1)} %pin_hbm.1, bf16[512,1024]{1,0:T(8,128)(2,1)} %pout_hbm.1, bf16[2,128,128]{2,1,0:T(8,128)(2,1)} %constant.10.clone.chan_hbm, bf16[128,128]{1,0:T(8,128)(2,1)} %constant.11.clone.unpack_hbm, ...), custom_call_target="tpu_custom_call" | custom-call | tf_op jit(solution)/shard_map/mix/pallas_call | solution.py:391
  41.6 1.4 %copy.10 = bf16[1152,1024]{1,0:T(8,128)(2,1)} copy(bf16[1152,1024]{1,0:T(8,128)(2,1)S(1)} %mix.1) | data formatting | bytes 4718592

commit v2 on v1

v2 whole, which is shorter than its diff:
```python
import functools
import math

import jax
import jax.numpy as jnp
import numpy as np
from jax import lax
from jax.experimental import pallas as pl
from jax.experimental.pallas import tpu as pltpu
from jax.sharding import PartitionSpec as P

MESH = pl.DeviceIdType.MESH


def up(value, step):
    return -(-value // step) * step


def plan(rows, devices):
    period = rows // 2
    piece = rows // (2 * devices)
    subs = 3 if piece % 24 == 0 else 1
    pad = up(piece // subs, 8)
    share = period // (2 * devices)
    height = up(share + 1, 8)
    packet = up(2 * share, 8)
    return period, piece, subs, pad, share, height, packet


@functools.lru_cache(maxsize=None)
def tables(rows, devices, group):
    period, piece, subs, pad, share, height, packet = plan(rows, devices)
    half = group // 2
    odd = np.arange(group) > half
    freq = np.where(odd, np.arange(group) - half, np.arange(group))
    angle = 2 * np.pi * (np.arange(group)[:, None] * freq[None, :] % group) / group
    chan = np.where(odd, np.sin(angle), np.cos(angle)) / math.sqrt(group)
    chan_hi = chan.astype(jnp.bfloat16)
    chan_lo = (chan - chan_hi.astype(np.float64)).astype(jnp.bfloat16)
    unpack = np.zeros((group, group))
    for col in range(group):
        f = freq[col]
        unpack[col, f] = -1.0 if odd[col] else 1.0
        unpack[col, (group - f) % group] = 1.0
    part = piece // subs
    pos = np.arange(2 * pad)
    is_y = pos >= pad
    local = np.where(is_y, pos - pad, pos)
    valid = np.tile(local < part, devices * subs)
    m = (part * np.arange(devices * subs)[:, None] + local[None, :]).reshape(-1)
    is_y = np.tile(is_y, devices * subs)
    k = share * np.arange(devices)[:, None] + np.arange(height)[None, :]
    seq = []
    for twice_m in (2 * m + is_y, 2 * np.where(is_y, period - 1 - m, m)):
        angle = np.pi * (twice_m[None, None, :] * k[:, :, None] % (2 * period)) / period
        both = np.stack([np.cos(angle), np.sin(angle)], axis=1) * valid
        seq.append(both.reshape(devices * 2 * height, -1))
    seq = np.stack(seq).astype(jnp.bfloat16)
    q = np.arange(2 * devices)[:, None]
    p = np.arange(devices)[None, :]
    angle = 2 * np.pi * (p * q % (2 * devices)) / (2 * devices)
    even_a, even_b = np.cos(angle), -np.sin(angle)
    odd_a, odd_b = np.sin(angle), np.cos(angle)
    for a, b in ((even_a, even_b), (odd_a, odd_b)):
        a[:, 0] = 1.0
        b[:, 0] = np.where(q[:, 0] % 2, -1.0, 1.0)
    coef = []
    for c in range(2):
        is_odd = odd[c * half:(c + 1) * half]
        first = np.where(is_odd, odd_a[:, :, None], even_a[:, :, None])
        second = np.where(is_odd, odd_b[:, :, None], even_b[:, :, None])
        coef.append(np.concatenate([first, second], axis=2))
    coef = np.stack(coef) / math.sqrt(rows * devices)
    perm = np.zeros((packet, 2 * height))
    for j in range(share):
        perm[j, j] = 1.0
        perm[share + j, height + share - j] = 1.0
    order = np.zeros((period, devices * packet))
    for row in range(period):
        if row < period // 2:
            order[row, row // share * packet + row % share] = 1.0
        else:
            s = (period - 1 - row) // share
            order[row, s * packet + share + row - (period - share * (s + 1))] = 1.0
    return (
        np.concatenate([chan_hi, chan_lo], axis=0),
        unpack.astype(jnp.bfloat16),
        seq,
        coef.astype(np.float32),
        perm.astype(jnp.bfloat16),
        order.astype(jnp.bfloat16),
    )


def cos_sin_small(x):
    square = x * x
    cos_sum, sin_sum = jnp.zeros_like(x), jnp.zeros_like(x)
    for j in range(8, -1, -1):
        sign = -1.0 if j % 2 else 1.0
        cos_sum = cos_sum * square + sign / math.factorial(2 * j)
        sin_sum = sin_sum * square + sign / math.factorial(2 * j + 1)
    return cos_sum, sin_sum * x


def kernel(
    devices, cols, chunks,
    tok_hbm, pin_hbm, pout_hbm, chan_hbm, unpack_hbm, seq_hbm, coef_hbm, perm_hbm, order_hbm,
    out_ref,
    tok, pin, pout, chan, unpack, seq, coef, perm, order,
    packed, send1, recv1, mid, send2, recv2, twc, tws, parts, send3, recv3, weight, acc,
    tok_sem, in_sem, ssem1, rsem1, ssem2, rsem2, ssem3, rsem3, gsem, ysem, psem,
):
    me = lax.axis_index("row")
    col = lax.axis_index("col")
    partner = col + 1 - 2 * lax.rem(col, 2)
    rows, group = packed.shape
    period, piece, subs, pad, share, height, packet = plan(rows, devices)
    half = group // 2
    f32, bf16 = jnp.float32, jnp.bfloat16
    chips = cols // 2
    wing = devices // 2

    def target(d):
        return lax.rem(me + 1 + d, devices)

    def source(d):
        return lax.rem(me + devices - 1 - d, devices)

    def peer_col(j):
        return lax.rem(col + 2 * j, cols)

    def each(body, count=devices - 1):
        def step(d, _):
            body(d)
            return 0

        lax.fori_loop(0, count, step, 0)

    barrier = pltpu.get_barrier_semaphore()

    step = rows // chunks
    depth = chunks // 2
    tok_copies = [
        pltpu.make_async_copy(
            tok_hbm.at[pl.ds(i * step, step)], tok.at[pl.ds(i * step, step)], tok_sem.at[i]
        )
        for i in range(chunks)
    ]
    loads = [
        pltpu.make_async_copy(src, dst, in_sem.at[i])
        for i, (src, dst) in enumerate(
            [
                (pin_hbm, pin),
                (chan_hbm, chan),
                (pout_hbm, pout),
                (unpack_hbm, unpack),
                (seq_hbm.at[jnp.minimum(me, 1)], seq),
                (coef_hbm, coef),
                (perm_hbm, perm),
                (order_hbm, order),
            ]
        )
    ]
    loads[0].start()
    tok_copies[0].start()
    loads[1].start()
    for copy in tok_copies[1:depth]:
        copy.start()
    each(lambda d: pl.semaphore_signal(
        barrier, inc=1, device_id={"row": target(d)}, device_id_type=MESH
    ))
    pl.semaphore_signal(barrier, inc=1, device_id={"col": partner}, device_id_type=MESH)
    for j in range(1, chips):
        pl.semaphore_signal(barrier, inc=1, device_id={"col": peer_col(j)}, device_id_type=MESH)

    lane = lax.broadcasted_iota(jnp.int32, (1, group), 1)
    low = lane < half

    shape = (devices, height, group)
    p_id = lax.broadcasted_iota(jnp.int32, shape, 0)
    k_id = lax.broadcasted_iota(jnp.int32, shape, 1) + share * me
    angle = (p_id * k_id).astype(f32) * (2.0 * math.pi / (rows * devices))
    cos_val, sin_val = cos_sin_small(angle)
    twc[...] = cos_val
    tws[...] = jnp.where(low, -sin_val, sin_val)

    def sign_of(channel):
        return jnp.where(channel > half, -1.0, 1.0).astype(f32)

    y_sign = sign_of(lane)

    def remote(src, dst, ssem, rsem, to):
        return pltpu.make_async_remote_copy(
            src_ref=src, dst_ref=dst, send_sem=ssem, recv_sem=rsem,
            device_id=to, device_id_type=MESH,
        )

    def exchange1(r, to, slot):
        return remote(
            send1.at[r, to], recv1.at[slot, r], ssem1.at[r, to], rsem1.at[r, slot], {"row": to}
        )

    part = piece // subs
    per_sub = chunks // subs
    if pad != part:
        send1[...] = jnp.zeros_like(send1)
    loads[0].wait()
    for i in range(chunks):
        tok_copies[i].wait()
        if i + depth < chunks:
            tok_copies[i + depth].start()
        elif i + depth == chunks:
            for copy in loads[2:]:
                copy.start()
        branch = jnp.dot(
            tok[i * step:(i + 1) * step, :], pin[...], preferred_element_type=f32
        ).astype(bf16)
        if i == 0:
            loads[1].wait()
        packed[i * step:(i + 1) * step, :] = jnp.dot(
            jnp.concatenate([branch, branch], axis=1), chan[...], preferred_element_type=f32
        )
        if (i + 1) % per_sub:
            continue
        r = i // per_sub
        base = r * (rows // subs)
        for p in range(devices):
            other = 2 * devices - p if p else devices
            y = packed[pl.ds(base + other, part, stride=2 * devices), :]
            if p:
                y = y * y_sign
            x = packed[pl.ds(base + p, part, stride=2 * devices), :]
            send1[r, p, 0, 0:part, :] = x.astype(bf16)
            send1[r, p, 1, 0:part, :] = y.astype(bf16)
        if r == 0:
            pl.semaphore_wait(barrier, devices - 1 + 1 + chips - 1)
        each(lambda d: exchange1(r, target(d), me).start())
    for r in range(subs):
        recv1[me, r] = send1[r, me]

    for copy in loads[2:]:
        copy.wait()
    for g in range(cols):
        unpacked = jnp.dot(
            unpack[...], pout[g * group:(g + 1) * group, :], preferred_element_type=f32
        ).astype(bf16)
        top = g // 2 * group
        for v in range(2):
            at = top + (half if (g + v) % 2 else 0)
            for c in range(2):
                weight[v, c, at:at + half, :] = unpacked[c * half:(c + 1) * half, :]

    first = me == 0

    def exchange2(c, to, slot):
        return remote(
            send2.at[c, to], recv2.at[c, slot], ssem2.at[c, to], rsem2.at[c, slot], {"row": to}
        )

    def channel_of(c):
        return c * half + lax.rem(lane, half)

    odd_lane = lane > half
    for r in range(subs):
        each(lambda d: exchange1(r, me, source(d)).wait_recv())
    data = recv1[...].reshape(devices * subs, 2, pad, group)
    blank = jnp.zeros_like(data[:, 0])
    flat = (devices * subs * 2 * pad, group)
    both = jnp.concatenate(
        [
            jnp.stack([data[:, 0], blank], axis=1).reshape(flat),
            jnp.stack([blank, data[:, 1]], axis=1).reshape(flat),
        ],
        axis=1,
    )
    mid[...] = jnp.dot(seq[...], both, preferred_element_type=f32).reshape(mid.shape)

    def fill(s):
        top_x, top_y = mid[s, :height, :group], mid[s, :height, group:]
        low_x, low_y = mid[s, height:, :group], mid[s, height:, group:]
        a = jnp.where(first, jnp.where(odd_lane, low_x, top_x), top_x + top_y)
        b = jnp.where(first, jnp.where(odd_lane, low_y, top_y), low_x + low_y)
        send2[0, s] = jnp.where(low, a, pltpu.roll(b, half, 1)).astype(bf16)
        send2[1, s] = jnp.where(low, pltpu.roll(a, half, 1), b).astype(bf16)

    def start2(d):
        fill(target(d))
        exchange2(0, target(d), me).start()

    each(start2)
    each(lambda d: exchange2(1, target(d), me).start())
    fill(me)
    recv2[0, me] = send2[0, me]
    recv2[1, me] = send2[1, me]

    def exchange3(c, to, slot):
        return remote(
            send3.at[c, to], recv3.at[c, col, slot], ssem3.at[c, to], rsem3.at[c, slot],
            {"row": to},
        )

    keep = jnp.logical_xor(low, lax.rem(col, 2) == 1)

    def combine(c):
        def rotate(src):
            value = recv2[c, src].astype(f32)
            parts[src] = twc[src] * value + tws[src] * pltpu.roll(value, half, 1)

        rotate(me)

        def arrive(d):
            exchange2(c, me, source(d)).wait_recv()
            rotate(source(d))

        each(arrive)
        sign = sign_of(channel_of(c))

        def outer(q):
            total = coef[c, q, 0][None, :] * parts[0]
            for p in range(1, devices):
                total = total + coef[c, q, p][None, :] * parts[p]
            return total

        def merge(one, two):
            return jnp.where(keep, one, two) + pltpu.roll(jnp.where(keep, two, one), half, 1)

        def pair(i):
            here = merge(outer(2 * i), outer(2 * i + 1))
            there = merge(outer(2 * devices - 1 - 2 * i), outer(2 * devices - 2 - 2 * i))
            stacked = jnp.concatenate(
                [
                    jnp.concatenate([here, there * sign], axis=0),
                    jnp.concatenate([there, here * sign], axis=0),
                ],
                axis=1,
            ).astype(bf16)
            moved = jnp.dot(perm[...], stacked, preferred_element_type=f32).astype(bf16)
            send3[c, i] = moved[:, :group]
            send3[c, devices - 1 - i] = moved[:, group:]

        if devices <= 8:
            for i in range(wing):
                pair(i)
        else:
            each(pair, wing)
        each(lambda d: exchange3(c, target(d), me).start())
        recv3[c, col, me] = send3[c, me]

    combine(0)
    combine(1)

    def to_partner(c, g, src):
        block = recv3.at[c, g, src]
        return remote(block, block, psem.at[g, src], gsem.at[c, g, src], {"col": partner})

    def to_chip(c, j, g, src):
        block = recv3.at[c, g, src]
        return remote(block, block, ysem.at[j, src], gsem.at[c, g, src], {"col": peer_col(j)})

    def forward(c, src):
        for j in range(1, chips):
            if c:
                to_chip(0, j, col, src).wait_send()
            to_chip(c, j, col, src).start()
        if c:
            to_partner(0, col, src).wait_send()
        to_partner(c, col, src).start()

    def relay(c, src):
        for j in range(1, chips):
            g = lax.rem(col + cols - 2 * j, cols)
            to_chip(c, j, g, src).wait_recv()
            if c:
                to_partner(0, g, src).wait_send()
            to_partner(c, g, src).start()

    def pass_on(c, src):
        exchange3(c, me, src).wait_recv()
        forward(c, src)

    def collect(c, src):
        for j in range(chips):
            to_partner(c, lax.rem(partner + 2 * j, cols), src).wait_recv()

    upper = me // wing
    mine = jnp.logical_xor(low, upper == 1)

    def finish(c, h):
        tiles = []
        for t in range(chips):
            one = recv3[c, 2 * t].reshape(devices * packet, group)
            two = recv3[c, 2 * t + 1].reshape(devices * packet, group)
            tiles.append(jnp.where(mine, two, one) if h else jnp.where(mine, one, two))
        arrived = jnp.concatenate(tiles, axis=1) if chips > 1 else tiles[0]
        natural = jnp.dot(order[...], arrived, preferred_element_type=f32).astype(bf16)
        which = 1 - upper if h else upper
        part = jnp.dot(natural, weight[which, c], preferred_element_type=f32)
        at = slice(h * period, (h + 1) * period)
        if c == 0:
            acc[at, :] = part
        else:
            out_ref[at, :] = (acc[at, :] + part).astype(bf16)

    forward(0, me)
    each(lambda d: pass_on(0, source(d)))
    forward(1, me)
    relay(0, me)

    def second(d):
        pass_on(1, source(d))
        relay(0, source(d))

    each(second)
    collect(0, me)
    each(lambda d: collect(0, source(d)))
    finish(0, 0)
    relay(1, me)
    each(lambda d: relay(1, source(d)))
    finish(0, 1)
    collect(1, me)
    each(lambda d: collect(1, source(d)))
    finish(1, 0)
    finish(1, 1)

    def drain(d):
        to = target(d)
        for r in range(subs):
            exchange1(r, to, me).wait_send()
        for c in range(2):
            exchange2(c, to, me).wait_send()
            exchange3(c, to, me).wait_send()

    each(drain)

    def drain_gather(src):
        for j in range(1, chips):
            to_chip(1, j, col, src).wait_send()
        for j in range(chips):
            to_partner(1, peer_col(j), src).wait_send()

    each(drain_gather, devices)


def solution(mesh):
    devices, cols = mesh.shape["row"], mesh.shape["col"]

    def on_device(tokens, proj_in, proj_out):
        rows, width = tokens.shape
        group = proj_in.shape[1]
        channels, out_cols = proj_out.shape
        period, piece, subs, pad, share, height, packet = plan(rows, devices)
        consts = tables(rows, devices, group)
        chunks = 6
        f32, bf16 = jnp.float32, jnp.bfloat16
        dma = pltpu.SemaphoreType.DMA
        operands = [tokens, proj_in, proj_out, *[jnp.asarray(c) for c in consts]]
        return pl.pallas_call(
            functools.partial(kernel, devices, cols, chunks),
            out_shape=jax.ShapeDtypeStruct((rows, out_cols), bf16),
            in_specs=[pl.BlockSpec(memory_space=pltpu.HBM)] * len(operands),
            out_specs=pl.BlockSpec(memory_space=pltpu.VMEM),
            scratch_shapes=[
                pltpu.VMEM((rows, width), bf16),
                pltpu.VMEM((width, group), bf16),
                pltpu.VMEM((channels, out_cols), bf16),
                pltpu.VMEM(consts[0].shape, bf16),
                pltpu.VMEM((group, group), bf16),
                pltpu.VMEM(consts[2].shape[1:], bf16),
                pltpu.VMEM(consts[3].shape, f32),
                pltpu.VMEM(consts[4].shape, bf16),
                pltpu.VMEM(consts[5].shape, bf16),
                pltpu.VMEM((rows, group), f32),
                pltpu.VMEM((subs, devices, 2, pad, group), bf16),
                pltpu.VMEM((devices, subs, 2, pad, group), bf16),
                pltpu.VMEM((devices, 2 * height, 2 * group), f32),
                pltpu.VMEM((2, devices, height, group), bf16),
                pltpu.VMEM((2, devices, height, group), bf16),
                pltpu.VMEM((devices, height, group), f32),
                pltpu.VMEM((devices, height, group), f32),
                pltpu.VMEM((devices, height, group), f32),
                pltpu.VMEM((2, devices, packet, group), bf16),
                pltpu.VMEM((2, cols, devices, packet, group), bf16),
                pltpu.VMEM((2, 2, channels // 2, out_cols), bf16),
                pltpu.VMEM((rows, out_cols), f32),
                dma((chunks,)),
                dma((8,)),
                dma((subs, devices)),
                dma((subs, devices)),
                dma((2, devices)),
                dma((2, devices)),
                dma((2, devices)),
                dma((2, devices)),
                dma((2, cols, devices)),
                dma((cols // 2, devices)),
                dma((cols, devices)),
            ],
            compiler_params=pltpu.CompilerParams(
                collective_id=0, has_side_effects=True, vmem_limit_bytes=44 * 2**20
            ),
            name="mix",
        )(*[pltpu.with_memory_space_constraint(a, pltpu.HBM) for a in operands])

    return jax.shard_map(
        on_device,
        mesh=mesh,
        in_specs=(P("row", None), P(None, "col"), P(None, "col")),
        out_specs=P("row", "col"),
        check_vma=False,
    )
```

time: 43.1 us -> 39.4 us (0.914)
  the two profiles are of different devices: /device:TPU:17 before, /device:TPU:0 now
where the time goes in v2:
time: 39.4 us; the launch traced here: 39.2 us
  Pallas kernels  37.8 us (96%)
  local copies, waits for them, and re-layouts  1.41 us (4%)
    pallas_call x1, Pallas kernels, on_device(): pl.pallas_call(functools.partial(kernel, devices, cols, chunks), out_shap...  37.8 us
    unnamed x1, local copies, waits for them, and re-layouts  1.41 us

profile of v2, /device:TPU:0, one launch (start us, length us, event | category | flops | bytes accessed | tf_op | source)
XLA Modules:
  0.0 39.2 jit_solution(11736913461098037006)
XLA Ops:
  0.0 37.8 %mix.1 = bf16[1152,1024]{1,0:T(8,128)(2,1)S(1)} custom-call(bf16[1152,4096]{1,0:T(8,128)(2,1)} %tok_hbm.1, bf16[4096,128]{1,0:T(8,128)(2,1)} %pin_hbm.1, bf16[512,1024]{1,0:T(8,128)(2,1)} %pout_hbm.1, bf16[256,128]{1,0:T(8,128)(2,1)} %constant.12.clone.chan_hbm, bf16[128,128]{1,0:T(8,128)(2,1)} %constant.13.clone.unpack_hbm, ...), custom_call_target="tpu_custom_call" | custom-call | tf_op jit(solution)/shard_map/mix/pallas_call | solution.py:457
  37.8 1.4 %copy.11 = bf16[1152,1024]{1,0:T(8,128)(2,1)} copy(bf16[1152,1024]{1,0:T(8,128)(2,1)S(1)} %mix.1) | data formatting | bytes 4718592

commit v3 on v2

--- a/solution.py
+++ b/solution.py
@@ -47,7 +47,11 @@
     is_y = pos >= pad
     local = np.where(is_y, pos - pad, pos)
     valid = np.tile(local < part, devices * subs)
-    m = (part * np.arange(devices * subs)[:, None] + local[None, :]).reshape(-1)
+    m = (
+        part * np.arange(subs)[:, None, None]
+        + piece * np.arange(devices)[None, :, None]
+        + local[None, None, :]
+    ).reshape(-1)
     is_y = np.tile(is_y, devices * subs)
     k = share * np.arange(devices)[:, None] + np.arange(height)[None, :]
     seq = []
@@ -108,7 +112,7 @@
     out_ref,
     tok, pin, pout, chan, unpack, seq, coef, perm, order,
     packed, send1, recv1, mid, send2, recv2, twc, tws, parts, send3, recv3, weight, acc,
-    tok_sem, in_sem, ssem1, rsem1, ssem2, rsem2, ssem3, rsem3, gsem, ysem, psem,
+    tok_sem, in_sem, ssem1, rsem1, ssem2, rsem2, ssem3, rsem3, gsem, ysem, nsem, psem,
 ):
     me = lax.axis_index("row")
     col = lax.axis_index("col")
@@ -128,6 +132,9 @@
 
     def peer_col(j):
         return lax.rem(col + 2 * j, cols)
+
+    def near(row):
+        return row // wing == me // wing
 
     def each(body, count=devices - 1):
         def step(d, _):
@@ -172,6 +179,17 @@
     pl.semaphore_signal(barrier, inc=1, device_id={"col": partner}, device_id_type=MESH)
     for j in range(1, chips):
         pl.semaphore_signal(barrier, inc=1, device_id={"col": peer_col(j)}, device_id_type=MESH)
+
+    def greet(d):
+        @pl.when(near(target(d)))
+        def _():
+            for j in range(1, chips):
+                pl.semaphore_signal(
+                    barrier, inc=1, device_id={"row": target(d), "col": peer_col(j)},
+                    device_id_type=MESH,
+                )
+
+    each(greet)
 
     lane = lax.broadcasted_iota(jnp.int32, (1, group), 1)
     low = lane < half
@@ -233,7 +251,7 @@
             send1[r, p, 0, 0:part, :] = x.astype(bf16)
             send1[r, p, 1, 0:part, :] = y.astype(bf16)
         if r == 0:
-            pl.semaphore_wait(barrier, devices - 1 + 1 + chips - 1)
+            pl.semaphore_wait(barrier, devices + (chips - 1) * wing)
         each(lambda d: exchange1(r, target(d), me).start())
     for r in range(subs):
         recv1[me, r] = send1[r, me]
@@ -261,19 +279,22 @@
         return c * half + lax.rem(lane, half)
 
     odd_lane = lane > half
+    span = devices * 2 * pad
     for r in range(subs):
         each(lambda d: exchange1(r, me, source(d)).wait_recv())
-    data = recv1[...].reshape(devices * subs, 2, pad, group)
-    blank = jnp.zeros_like(data[:, 0])
-    flat = (devices * subs * 2 * pad, group)
-    both = jnp.concatenate(
-        [
-            jnp.stack([data[:, 0], blank], axis=1).reshape(flat),
-            jnp.stack([blank, data[:, 1]], axis=1).reshape(flat),
-        ],
-        axis=1,
-    )
-    mid[...] = jnp.dot(seq[...], both, preferred_element_type=f32).reshape(mid.shape)
+        data = recv1[:, r]
+        blank = jnp.zeros_like(data[:, 0])
+        both = jnp.concatenate(
+            [
+                jnp.stack([data[:, 0], blank], axis=1).reshape(span, group),
+                jnp.stack([blank, data[:, 1]], axis=1).reshape(span, group),
+            ],
+            axis=1,
+        )
+        term = jnp.dot(
+            seq[:, r * span:(r + 1) * span], both, preferred_element_type=f32
+        ).reshape(mid.shape)
+        mid[...] = mid[...] + term if r else term
 
     def fill(s):
         top_x, top_y = mid[s, :height, :group], mid[s, :height, group:]
@@ -297,6 +318,12 @@
         return remote(
             send3.at[c, to], recv3.at[c, col, slot], ssem3.at[c, to], rsem3.at[c, slot],
             {"row": to},
+        )
+
+    def direct(c, j, to):
+        return remote(
+            send3.at[c, to], recv3.at[c, col, me], nsem.at[j, to], gsem.at[c, col, me],
+            {"row": to, "col": peer_col(j)},
         )
 
     keep = jnp.logical_xor(low, lax.rem(col, 2) == 1)
@@ -343,7 +370,19 @@
                 pair(i)
         else:
             each(pair, wing)
-        each(lambda d: exchange3(c, target(d), me).start())
+
+        def start3(d):
+            to = target(d)
+            exchange3(c, to, me).start()
+
+            @pl.when(near(to))
+            def _():
+                for j in range(1, chips):
+                    if c:
+                        direct(0, j, to).wait_send()
+                    direct(c, j, to).start()
+
+        each(start3)
         recv3[c, col, me] = send3[c, me]
 
     combine(0)
@@ -358,10 +397,13 @@
         return remote(block, block, ysem.at[j, src], gsem.at[c, g, src], {"col": peer_col(j)})
 
     def forward(c, src):
-        for j in range(1, chips):
-            if c:
-                to_chip(0, j, col, src).wait_send()
-            to_chip(c, j, col, src).start()
+        @pl.when(jnp.logical_or(src == me, jnp.logical_not(near(src))))
+        def _():
+            for j in range(1, chips):
+                if c:
+                    to_chip(0, j, col, src).wait_send()
+                to_chip(c, j, col, src).start()
+
         if c:
             to_partner(0, col, src).wait_send()
         to_partner(c, col, src).start()
@@ -433,8 +475,18 @@
     each(drain)
 
     def drain_gather(src):
-        for j in range(1, chips):
-            to_chip(1, j, col, src).wait_send()
+        aside = jnp.logical_and(src != me, near(src))
+
+        @pl.when(jnp.logical_not(aside))
+        def _():
+            for j in range(1, chips):
+                to_chip(1, j, col, src).wait_send()
+
+        @pl.when(aside)
+        def _():
+            for j in range(1, chips):
+                direct(1, j, src).wait_send()
+
         for j in range(chips):
             to_partner(1, peer_col(j), src).wait_send()
 
@@ -492,6 +544,7 @@
                 dma((2, devices)),
                 dma((2, cols, devices)),
                 dma((cols // 2, devices)),
+                dma((cols // 2, devices)),
                 dma((cols, devices)),
             ],
             compiler_params=pltpu.CompilerParams(

time: 39.4 us -> 38.9 us (0.987)
  Pallas kernels: 37.8 us -> 37.3 us
    pallas_call x1, Pallas kernels: 37.8 us -> 37.3 us  [on_device(): pl.pallas_call(functools.partial(kernel, devices, cols, chunks), out_shap...]
where the time goes in v3:
time: 38.9 us; the launch traced here: 38.7 us
  Pallas kernels  37.3 us (96%)
  local copies, waits for them, and re-layouts  1.41 us (4%)
    pallas_call x1, Pallas kernels, on_device(): pl.pallas_call(functools.partial(kernel, devices, cols, chunks), out_shap...  37.3 us
    unnamed x1, local copies, waits for them, and re-layouts  1.41 us

profile of v3, /device:TPU:0, one launch (start us, length us, event | category | flops | bytes accessed | tf_op | source)
XLA Modules:
  0.0 38.7 jit_solution(8546051069212982109)
XLA Ops:
  0.0 37.3 %mix.1 = bf16[1152,1024]{1,0:T(8,128)(2,1)S(1)} custom-call(bf16[1152,4096]{1,0:T(8,128)(2,1)} %tok_hbm.1, bf16[4096,128]{1,0:T(8,128)(2,1)} %pin_hbm.1, bf16[512,1024]{1,0:T(8,128)(2,1)} %pout_hbm.1, bf16[256,128]{1,0:T(8,128)(2,1)} %constant.12.clone.chan_hbm, bf16[128,128]{1,0:T(8,128)(2,1)} %constant.13.clone.unpack_hbm, ...), custom_call_target="tpu_custom_call" | custom-call | tf_op jit(solution)/shard_map/mix/pallas_call | solution.py:509
  37.3 1.4 %copy.11 = bf16[1152,1024]{1,0:T(8,128)(2,1)} copy(bf16[1152,1024]{1,0:T(8,128)(2,1)S(1)} %mix.1) | data formatting | bytes 4718592

commit v4 on v3

--- a/solution.py
+++ b/solution.py
@@ -79,20 +79,12 @@
     for j in range(share):
         perm[j, j] = 1.0
         perm[share + j, height + share - j] = 1.0
-    order = np.zeros((period, devices * packet))
-    for row in range(period):
-        if row < period // 2:
-            order[row, row // share * packet + row % share] = 1.0
-        else:
-            s = (period - 1 - row) // share
-            order[row, s * packet + share + row - (period - share * (s + 1))] = 1.0
     return (
         np.concatenate([chan_hi, chan_lo], axis=0),
         unpack.astype(jnp.bfloat16),
         seq,
         coef.astype(np.float32),
         perm.astype(jnp.bfloat16),
-        order.astype(jnp.bfloat16),
     )
 
 
@@ -108,9 +100,9 @@
 
 def kernel(
     devices, cols, chunks,
-    tok_hbm, pin_hbm, pout_hbm, chan_hbm, unpack_hbm, seq_hbm, coef_hbm, perm_hbm, order_hbm,
+    tok_hbm, pin_hbm, pout_hbm, chan_hbm, unpack_hbm, seq_hbm, coef_hbm, perm_hbm,
     out_ref,
-    tok, pin, pout, chan, unpack, seq, coef, perm, order,
+    tok, pin, pout, chan, unpack, seq, coef, perm,
     packed, send1, recv1, mid, send2, recv2, twc, tws, parts, send3, recv3, weight, acc,
     tok_sem, in_sem, ssem1, rsem1, ssem2, rsem2, ssem3, rsem3, gsem, ysem, nsem, psem,
 ):
@@ -136,12 +128,12 @@
     def near(row):
         return row // wing == me // wing
 
-    def each(body, count=devices - 1):
+    def each(body, count=devices - 1, unroll=False):
         def step(d, _):
             body(d)
             return 0
 
-        lax.fori_loop(0, count, step, 0)
+        lax.fori_loop(0, count, step, 0, unroll=unroll)
 
     barrier = pltpu.get_barrier_semaphore()
 
@@ -164,7 +156,6 @@
                 (seq_hbm.at[jnp.minimum(me, 1)], seq),
                 (coef_hbm, coef),
                 (perm_hbm, perm),
-                (order_hbm, order),
             ]
         )
     ]
@@ -308,7 +299,7 @@
         fill(target(d))
         exchange2(0, target(d), me).start()
 
-    each(start2)
+    each(start2, unroll=devices <= 8)
     each(lambda d: exchange2(1, target(d), me).start())
     fill(me)
     recv2[0, me] = send2[0, me]
@@ -339,7 +330,7 @@
             exchange2(c, me, source(d)).wait_recv()
             rotate(source(d))
 
-        each(arrive)
+        each(arrive, unroll=devices <= 8)
         sign = sign_of(channel_of(c))
 
         def outer(q):
@@ -427,21 +418,30 @@
     upper = me // wing
     mine = jnp.logical_xor(low, upper == 1)
 
-    def finish(c, h):
+    def finish(c):
         tiles = []
-        for t in range(chips):
-            one = recv3[c, 2 * t].reshape(devices * packet, group)
-            two = recv3[c, 2 * t + 1].reshape(devices * packet, group)
-            tiles.append(jnp.where(mine, two, one) if h else jnp.where(mine, one, two))
-        arrived = jnp.concatenate(tiles, axis=1) if chips > 1 else tiles[0]
-        natural = jnp.dot(order[...], arrived, preferred_element_type=f32).astype(bf16)
-        which = 1 - upper if h else upper
-        part = jnp.dot(natural, weight[which, c], preferred_element_type=f32)
-        at = slice(h * period, (h + 1) * period)
-        if c == 0:
-            acc[at, :] = part
-        else:
-            out_ref[at, :] = (acc[at, :] + part).astype(bf16)
+        for h in range(2):
+            for t in range(chips):
+                one = recv3[c, 2 * t].reshape(devices * packet, group)
+                two = recv3[c, 2 * t + 1].reshape(devices * packet, group)
+                tiles.append(jnp.where(mine, two, one) if h else jnp.where(mine, one, two))
+        lined = jnp.concatenate(tiles, axis=1).astype(f32).reshape(devices, packet, -1)
+        natural = jnp.concatenate(
+            [lined[p, :share] for p in range(devices)]
+            + [lined[p, share:2 * share] for p in range(devices - 1, -1, -1)],
+            axis=0,
+        ).astype(bf16)
+        for h in range(2):
+            which = 1 - upper if h else upper
+            part = jnp.dot(
+                natural[:, h * chips * group:(h + 1) * chips * group], weight[which, c],
+                preferred_element_type=f32,
+            )
+            at = slice(h * period, (h + 1) * period)
+            if c == 0:
+                acc[at, :] = part
+            else:
+                out_ref[at, :] = (acc[at, :] + part).astype(bf16)
 
     forward(0, me)
     each(lambda d: pass_on(0, source(d)))
@@ -455,14 +455,12 @@
     each(second)
     collect(0, me)
     each(lambda d: collect(0, source(d)))
-    finish(0, 0)
+    finish(0)
     relay(1, me)
     each(lambda d: relay(1, source(d)))
-    finish(0, 1)
     collect(1, me)
     each(lambda d: collect(1, source(d)))
-    finish(1, 0)
-    finish(1, 1)
+    finish(1)
 
     def drain(d):
         to = target(d)
@@ -520,7 +518,6 @@
                 pltpu.VMEM(consts[2].shape[1:], bf16),
                 pltpu.VMEM(consts[3].shape, f32),
                 pltpu.VMEM(consts[4].shape, bf16),
-                pltpu.VMEM(consts[5].shape, bf16),
                 pltpu.VMEM((rows, group), f32),
                 pltpu.VMEM((subs, devices, 2, pad, group), bf16),
                 pltpu.VMEM((devices, subs, 2, pad, group), bf16),
@@ -535,7 +532,7 @@
                 pltpu.VMEM((2, 2, channels // 2, out_cols), bf16),
                 pltpu.VMEM((rows, out_cols), f32),
                 dma((chunks,)),
-                dma((8,)),
+                dma((7,)),
                 dma((subs, devices)),
                 dma((subs, devices)),
                 dma((2, devices)),

time: 38.9 us -> 37.8 us (0.972)
  Pallas kernels: 37.3 us -> 36.1 us
    pallas_call x1, Pallas kernels: 37.3 us -> 36.1 us  [on_device(): pl.pallas_call(functools.partial(kernel, devices, cols, chunks), out_shap...]
where the time goes in v4:
time: 37.8 us; the launch traced here: 37.5 us
  Pallas kernels  36.1 us (96%)
  local copies, waits for them, and re-layouts  1.41 us (4%)
    pallas_call x1, Pallas kernels, on_device(): pl.pallas_call(functools.partial(kernel, devices, cols, chunks), out_shap...  36.1 us
    unnamed x1, local copies, waits for them, and re-layouts  1.41 us

profile of v4, /device:TPU:0, one launch (start us, length us, event | category | flops | bytes accessed | tf_op | source)
XLA Modules:
  0.0 37.5 jit_solution(3154894485572195394)
XLA Ops:
  0.0 36.1 %mix.1 = bf16[1152,1024]{1,0:T(8,128)(2,1)S(1)} custom-call(bf16[1152,4096]{1,0:T(8,128)(2,1)} %tok_hbm.1, bf16[4096,128]{1,0:T(8,128)(2,1)} %pin_hbm.1, bf16[512,1024]{1,0:T(8,128)(2,1)} %pout_hbm.1, bf16[256,128]{1,0:T(8,128)(2,1)} %constant.10.clone.chan_hbm, bf16[128,128]{1,0:T(8,128)(2,1)} %constant.11.clone.unpack_hbm, ...), custom_call_target="tpu_custom_call" | custom-call | tf_op jit(solution)/shard_map/mix/pallas_call | solution.py:507
  36.1 1.4 %copy.10 = bf16[1152,1024]{1,0:T(8,128)(2,1)} copy(bf16[1152,1024]{1,0:T(8,128)(2,1)S(1)} %mix.1) | data formatting | bytes 4718592

commit v5 on v4

--- a/solution.py
+++ b/solution.py
@@ -249,15 +249,19 @@
 
     for copy in loads[2:]:
         copy.wait()
-    for g in range(cols):
-        unpacked = jnp.dot(
-            unpack[...], pout[g * group:(g + 1) * group, :], preferred_element_type=f32
-        ).astype(bf16)
-        top = g // 2 * group
-        for v in range(2):
-            at = top + (half if (g + v) % 2 else 0)
-            for c in range(2):
-                weight[v, c, at:at + half, :] = unpacked[c * half:(c + 1) * half, :]
+
+    def mix_weight(t):
+        for b in range(2):
+            g_at = pl.ds(pl.multiple_of((2 * t + b) * group, group), group)
+            unpacked = jnp.dot(
+                unpack[...], pout[g_at, :], preferred_element_type=f32
+            ).astype(bf16)
+            for v in range(2):
+                at = pl.ds(pl.multiple_of(t * group + half * ((b + v) % 2), half), half)
+                for c in range(2):
+                    weight[v, c, at, :] = unpacked[c * half:(c + 1) * half, :]
+
+    each(mix_weight, chips)
 
     first = me == 0
 
@@ -299,7 +303,7 @@
         fill(target(d))
         exchange2(0, target(d), me).start()
 
-    each(start2, unroll=devices <= 8)
+    each(start2)
     each(lambda d: exchange2(1, target(d), me).start())
     fill(me)
     recv2[0, me] = send2[0, me]
@@ -330,7 +334,7 @@
             exchange2(c, me, source(d)).wait_recv()
             rotate(source(d))
 
-        each(arrive, unroll=devices <= 8)
+        each(arrive)
         sign = sign_of(channel_of(c))
 
         def outer(q):

time: 37.8 us -> 37.8 us (level)
  no operation moved by 1% of the time
where the time goes in v5:
time: 37.8 us; the launch traced here: 37.5 us
  Pallas kernels  36.1 us (96%)
  local copies, waits for them, and re-layouts  1.41 us (4%)
    pallas_call x1, Pallas kernels, on_device(): pl.pallas_call(functools.partial(kernel, devices, cols, chunks), out_shap...  36.1 us
    unnamed x1, local copies, waits for them, and re-layouts  1.41 us

profile of v5, /device:TPU:0, one launch (start us, length us, event | category | flops | bytes accessed | tf_op | source)
XLA Modules:
  0.0 37.5 jit_solution(10944050015336040412)
XLA Ops:
  0.0 36.1 %mix.1 = bf16[1152,1024]{1,0:T(8,128)(2,1)S(1)} custom-call(bf16[1152,4096]{1,0:T(8,128)(2,1)} %tok_hbm.1, bf16[4096,128]{1,0:T(8,128)(2,1)} %pin_hbm.1, bf16[512,1024]{1,0:T(8,128)(2,1)} %pout_hbm.1, bf16[256,128]{1,0:T(8,128)(2,1)} %constant.10.clone.chan_hbm, bf16[128,128]{1,0:T(8,128)(2,1)} %constant.11.clone.unpack_hbm, ...), custom_call_target="tpu_custom_call" | custom-call | tf_op jit(solution)/shard_map/mix/pallas_call | solution.py:511
  36.1 1.4 %copy.10 = bf16[1152,1024]{1,0:T(8,128)(2,1)} copy(bf16[1152,1024]{1,0:T(8,128)(2,1)S(1)} %mix.1) | data formatting | bytes 4718592
